TPU v7x, 32 devices: a whole 2x2x4 slice. The times are simulated.
32 devices in a mesh: sp: 16 (over z, y, x), tp: 2 (over core).
Axes of the slice: x: 2, y: 2, z: 4, core: 2. Of those that a mesh axis runs over, the one named last changes fastest.
Arguments:
- residual: bfloat16 [4096, 2048], P('sp'), may hold values from -6 to 6
- queries: bfloat16 [4096, 1024], P('sp', 'tp'), may hold values from -6 to 6
- forget_gate_logits: bfloat16 [4096, 1024], P('sp', 'tp'), may hold values from -5 to 5
- projected_values: bfloat16 [4096, 1024], P('sp', 'tp'), may hold values from -6 to 6
- output_gate_logits: bfloat16 [4096, 1024], P('sp', 'tp'), may hold values from -6 to 6
- lower_bound_margin: float32 [1024], P('tp'), may hold values from 0.00024414062 to 0.08
- extra_forget_logs: float32 [4096, 1024], P('sp', 'tp'), may hold values from -0.7 to 0
- per_head_norm_gain: float32 [128], replicated, may hold values from 0.1 to 1.9
- output_weight: bfloat16 [1024, 2048], P('tp'), may hold values from -0.1875 to 0.1875
- feedforward_norm_gain: float32 [2048], replicated, may hold values from 0.1 to 1.9
- gate_weight: bfloat16 [2048, 5632], P('sp', 'tp'), may hold values from -0.125 to 0.125
- up_weight: bfloat16 [2048, 5632], P('sp', 'tp'), may hold values from -0.125 to 0.125
- down_weight: bfloat16 [5632, 2048], P('tp', 'sp'), may hold values from -0.078125 to 0.078125
Outputs:
- layer_out: bfloat16 [4096, 2048], P('sp')
All inputs are finite; a program needn't handle non-finite values.
Results may differ from a plain program's by a relative error of at most 0.015.
Values may be sent and summed in bfloat16 or wider, within the bound.
A program may use at most 128 MiB of HBM per device.

v0:
```python
import jax
import jax.numpy as jnp
from jax import lax
from jax.experimental import pallas as pl
from jax.experimental.pallas import tpu as pltpu
from jax.sharding import PartitionSpec as P

HD = 128
BLOCK = 64


eps = 1e-06
top_precision = lax.Precision.HIGHEST


def carried_in_2(value, axis, join, neutral):
    place = lax.axis_index(axis)
    gathered = jax.tree.map(
        lambda a, kind: lax.all_gather(a.astype(kind), axis), value, (jnp.bfloat16, jnp.bfloat16)
    )
    state = jax.tree.map(lambda a, e: jnp.zeros_like(a) + jnp.asarray(e, a.dtype), value, neutral)

    def one(turn, state):
        return join(
            state,
            jax.tree.map(
                lambda a, own: lax.dynamic_index_in_dim(a, turn, 0, False).astype(own.dtype),
                gathered,
                value,
            ),
        )

    return lax.fori_loop(0, place, one, state)


def block_update(carried_in, inputs):
    recurrent_state, offset = carried_in
    queries, state_increment, value_rows, retain_log_factor = inputs
    running_state = jnp.cumsum(retain_log_factor, axis=1)
    causal = jnp.tril(
        jnp.ones((retain_log_factor.shape[1], retain_log_factor.shape[1]), dtype=bool)
    )
    carried_over_state = jnp.einsum(
        "uqw,uwa->uqa", queries * jnp.exp(running_state), recurrent_state, precision=top_precision
    )
    spread = running_state[:, :, None, :] - running_state[:, None, :, :]
    weights = jnp.exp(jnp.where(causal[None, :, :, None], spread, -jnp.inf))
    scores = jnp.einsum(
        "htk,htsk,hsk->hts", queries, weights, state_increment, precision=top_precision
    )
    output_rows = carried_over_state + jnp.einsum(
        "hts,hsv->htv", scores, value_rows, precision=top_precision
    )
    final_state = running_state[:, -1:, :]
    updated_state = jnp.exp(final_state[:, 0, :])[:, :, None] * recurrent_state + jnp.einsum(
        "erb,erc->ebc",
        state_increment * jnp.exp(final_state - running_state),
        value_rows,
        precision=top_precision,
    )
    rescaled_state = queries * jnp.exp(running_state + offset[:, None, :])
    return ((updated_state, offset + final_state[:, 0, :]), (output_rows, rescaled_state))


def join_states(earlier, later):
    earlier_sum, earlier_memory = earlier
    later_sum, later_memory = later
    return (earlier_sum + later_sum, jnp.exp(later_sum)[:, :, None] * earlier_memory + later_memory)


MESH = pl.DeviceIdType.MESH
GROUPS = 4


def up_to(value, step):
    return -(-value // step) * step


def layer_kernel(
    dims, gu_ref, dn_ref, q_ref, f_ref, v_ref, og_ref, margin_ref, extra_ref, head_gain_ref, ow_ref,
    residual_ref, ff_gain_ref, out_ref,
    gu, dn, grown, q_grown, plane, columns, gated, proj, proj_got, x_own, rows_in, hid, part, peer_part, summed, got,
    s_a, r_a, s_b, r_b, s_x, r_x, s_p, r_p, s_d, r_d, s_r, r_r, s_o, r_o, s_l,
    s_1, r_1, s_2, r_2, s_j, r_j,
):
    n_r, share, own, width, padded = dims
    me = lax.axis_index("sp")
    c = lax.axis_index("tp")
    h, r = me // n_r, me % n_r
    model = gu.shape[0]

    def away(d):
        return (h + d) % GROUPS

    def back(d):
        return (h + GROUPS - d) % GROUPS

    def beside(e):
        return ((r // 2 + e // 2) % 2) * 2 + (r % 2 + e % 2) % 2

    def remote(src, dst, send, recv, hh, rr, cc):
        return pltpu.make_async_remote_copy(
            src_ref=src, dst_ref=dst, send_sem=send, recv_sem=recv,
            device_id=(hh * n_r + rr, cc), device_id_type=MESH,
        )

    def gu_rows(owner):
        return gu.at[pl.ds(pl.multiple_of(owner * share, share), share)]

    def dn_cols(owner):
        return dn.at[pl.ds(0, width), pl.ds(pl.multiple_of(owner * share, share), share)]

    def token_rows(hh, cc):
        return pl.ds(pl.multiple_of((hh * 2 + cc) * own, own), own)

    started = []

    def go(copy):
        copy.start()
        started.append(copy)
        return copy

    weights_a = {}
    weights_b = {}
    mine = pl.ds(pl.multiple_of(c * own, own), own)
    theirs = pl.ds(pl.multiple_of((1 - c) * own, own), own)

    def share_out(k):
        source = (gu_ref, dn_ref)[k]
        place = (gu_rows, dn_cols)[k]
        for d in (1, 3, 2):
            weights_a[d, k] = go(remote(source.at[away(d)], place(me), s_a.at[d - 1, k], r_a.at[d - 1, k], away(d), r, c))
        for e in (1, 2):
            weights_b[0, e, k] = go(remote(source.at[h], place(me), s_b.at[0, e - 1, k], r_b.at[0, e - 1, k], h, beside(e), c))

    def hand_on(d, k):
        weights_a[d, k].wait_recv()
        block = (gu_rows, dn_cols)[k](back(d) * n_r + r)
        for e in (1, 2):
            weights_b[d, e, k] = go(remote(block, block, s_b.at[d, e - 1, k], r_b.at[d, e - 1, k], h, beside(e), c))

    here_already = set()

    def arrive(*key):
        if key not in here_already:
            here_already.add(key)
            weights_b[key].wait_recv()

    def relay(d, k):
        first = 1 + d % 2
        arrive(d, first, k)
        block = (gu_rows, dn_cols)[k](back(d) * n_r + beside(first))
        weights_b[d, 3, k] = go(remote(block, block, s_b.at[d, 2, k], r_b.at[d, 2, k], h, beside(3 - first), c))

    share_out(0)
    own_gu = pltpu.make_async_copy(gu_ref.at[h], gu_rows(me), s_l.at[0])
    own_dn = pltpu.make_async_copy(dn_ref.at[h], dn_cols(me), s_l.at[1])
    own_gu.start()
    own_dn.start()
    if padded > width:
        dn[pl.ds(width, padded - width), :] = jnp.zeros((padded - width, model), dn.dtype)

    bf, f32 = jnp.bfloat16, jnp.float32
    length, channels = q_ref.shape
    heads = channels // HD
    span = 128
    ones = lambda n: lax.broadcasted_iota(jnp.int32, (n, n), 0) >= lax.broadcasted_iota(jnp.int32, (n, n), 1)
    lower = ones(length).astype(f32)
    causal = ones(span)
    over = lambda x, y, i, j: lax.dot_general(x, y, (((i,), (j,)), ((), ())), preferred_element_type=f32)
    for n in range(heads):
        cols = slice(n * HD, (n + 1) * HD)
        inflow = margin_ref[:, cols] * jax.nn.sigmoid(-f_ref[:, cols].astype(f32))
        keep = jnp.log1p(-inflow) + extra_ref[:, cols]
        total_log = lax.dot_general(lower, keep, (((1,), (0,)), ((), ())), precision=top_precision, preferred_element_type=f32)
        q = q_ref[:, cols].astype(f32)
        q_grown[:, cols] = (q * jnp.exp(total_log)).astype(bf)
        state = None
        for start in range(0, length, span):
            rows = slice(start, start + span)
            a, qb, ub, vb = total_log[rows], q[rows], inflow[rows], v_ref[rows, cols]
            middle, end = a[span // 2 - 1:span // 2], a[span - 1:span]
            scores = over((qb * jnp.exp(a - middle)).astype(bf), (ub * jnp.exp(middle - a)).astype(bf), 1, 1)
            mixed = over(jnp.where(causal, scores, 0.0).astype(bf), vb, 1, 0)
            added = over(vb, (ub * jnp.exp(end - a)).astype(bf), 0, 0)
            if state is None:
                state = added
            else:
                mixed = mixed + over((qb * jnp.exp(a - base)).astype(bf), state.astype(bf), 1, 1)
                state = state * jnp.exp(end - base) + added
            grown[rows, cols] = mixed
            base = end
        plane[r, n * HD:(n + 1) * HD, :] = state.astype(bf)
        high = base.astype(bf)
        plane[r, heads * HD + n:heads * HD + n + 1, :] = high
        plane[r, heads * HD + 8 + n:heads * HD + 9 + n, :] = (base - high.astype(f32)).astype(bf)

    across = {e: go(remote(plane.at[r], plane.at[r], s_1.at[e - 1], r_1.at[e - 1], h, beside(e), c)) for e in (1, 2, 3)}
    relay(0, 0)
    hand_on(1, 0)
    for e in (1, 2, 3):
        across[e].wait_recv()

    def part_of(ref, at, n):
        logs = ref[at, heads * HD + n:heads * HD + n + 1, :].astype(f32) + ref[at, heads * HD + 8 + n:heads * HD + 9 + n, :].astype(f32)
        return logs, ref[at, n * HD:(n + 1) * HD, :].astype(f32)

    before = []
    for n in range(heads):
        whole = jnp.zeros((HD, HD), f32)
        whole_log = jnp.zeros((1, HD), f32)
        early, early_log = whole, whole_log
        for at in range(n_r):
            logs, state = part_of(plane, at, n)
            whole = whole * jnp.exp(logs) + state
            whole_log = whole_log + logs
            early = jnp.where(at < r, whole, early)
            early_log = jnp.where(at < r, whole_log, early_log)
        before.append((early_log, early))
        columns[h, n * HD:(n + 1) * HD, :] = whole.astype(bf)
        high = whole_log.astype(bf)
        columns[h, heads * HD + n:heads * HD + n + 1, :] = high
        columns[h, heads * HD + 8 + n:heads * HD + 9 + n, :] = (whole_log - high.astype(f32)).astype(bf)
    along = {d: go(remote(columns.at[h], columns.at[h], s_2.at[d - 1], r_2.at[d - 1], away(d), r, c)) for d in (1, 3, 2)}
    hand_on(3, 0)
    relay(1, 0)
    hand_on(2, 0)
    share_out(1)
    for d in (1, 3, 2):
        along[d].wait_recv()
    for n in range(heads):
        cols = slice(n * HD, (n + 1) * HD)
        state = jnp.zeros((HD, HD), f32)
        for at in range(GROUPS - 1):
            logs, later = part_of(columns, at, n)
            state = jnp.where(at < h, state * jnp.exp(logs) + later, state)
        early_log, early = before[n]
        state = state * jnp.exp(early_log) + early
        mixed = grown[:, cols] + over(q_grown[:, cols], state.astype(bf), 1, 1)
        scale = lax.rsqrt(jnp.mean(mixed * mixed, axis=-1, keepdims=True) + eps)
        gate = og_ref[:, cols].astype(f32)
        gated[:, cols] = (mixed * scale * head_gain_ref[...] * (gate * jax.nn.sigmoid(gate))).astype(bf)

    def project(j, carry):
        at = pl.multiple_of(j * 256, 256)
        proj[:, pl.ds(at, 256)] = jnp.dot(
            gated[...], ow_ref[:, pl.ds(at, 256)], preferred_element_type=f32
        ).astype(bf)
        return carry

    lax.fori_loop(0, model // 256, project, 0)
    joined = go(remote(proj.at[theirs], proj_got, s_j.at[0], r_j.at[0], h, r, 1 - c))
    joined.wait_recv()
    x = (residual_ref[mine, :].astype(f32) + (proj[mine, :].astype(f32) + proj_got[...].astype(f32))).astype(bf)
    x_own[...] = x
    wide = x.astype(f32)
    normed = wide * lax.rsqrt(jnp.mean(wide * wide, axis=-1, keepdims=True) + eps) * ff_gain_ref[...]
    rows_in[token_rows(h, c), :] = normed.astype(bf)
    block = rows_in.at[token_rows(h, c)]
    acts = {d: go(remote(block, block, s_x.at[d - 1], r_x.at[d - 1], away(d), r, c)) for d in (1, 3, 2)}
    peers = {0: go(remote(block, block, s_p.at[0], r_p.at[0], h, r, 1 - c))}
    relay(3, 0)
    hand_on(1, 1)
    relay(2, 0)
    hand_on(3, 1)
    relay(0, 1)
    hand_on(2, 1)
    for d in (1, 3, 2):
        relay(d, 1)
    for d in (1, 3, 2):
        acts[d].wait_recv()
        block = rows_in.at[token_rows(back(d), c)]
        peers[d] = go(remote(block, block, s_p.at[d], r_p.at[d], h, r, 1 - c))
    own_gu.wait()
    own_dn.wait()
    for d in range(4):
        for e in (1, 2, 3):
            arrive(d, e, 0)

    def reduce_block(d, exchange):
        exchange.wait_recv()
        here = part[d, mine, :]
        total = here.astype(jnp.float32) + peer_part[d].astype(jnp.float32)
        summed[d] = total.astype(jnp.bfloat16)
        if d == 0:
            return None
        return go(remote(summed.at[d], got.at[d - 1], s_r.at[d - 1], r_r.at[d - 1], back(d), r, c))

    tile = 256
    order = (1, 3, 2, 0)
    exchanges = {}
    reduced = {}
    for place, d in enumerate(order):
        peers[d].wait_recv()
        first = pl.multiple_of(back(d) * 2 * own, 2 * own)

        def gate_up(j, carry):
            at = pl.multiple_of(j * 256, 256)
            both = jnp.dot(rows_in[pl.ds(first, 2 * own), :], gu[:, pl.ds(at, 256)], preferred_element_type=jnp.float32)
            gate, up = both[:, :128], both[:, 128:]
            hid[:, pl.ds(pl.multiple_of(j * 128, 128), 128)] = (gate * jax.nn.sigmoid(gate) * up).astype(jnp.bfloat16)
            return carry

        lax.fori_loop(0, width // 128, gate_up, 0)
        if width % 128:
            both = jnp.dot(
                rows_in[pl.ds(first, 2 * own), :], gu[:, 2 * (width // 128 * 128):], preferred_element_type=jnp.float32
            )
            hid[:, width // 128 * 128:] = (both * jax.nn.sigmoid(both) * pltpu.roll(both, 64, 1)).astype(jnp.bfloat16)
        if place == 0:
            for dd in range(4):
                for e in (1, 2, 3):
                    arrive(dd, e, 1)

        def down(j, carry):
            at = pl.multiple_of(j * tile, tile)
            part[d, :, pl.ds(at, tile)] = jnp.dot(
                hid[...], dn[:, pl.ds(at, tile)], preferred_element_type=jnp.float32
            ).astype(jnp.bfloat16)
            return carry

        lax.fori_loop(0, model // tile, down, 0)
        exchanges[d] = go(remote(
            part.at[d, theirs], peer_part.at[d],
            s_d.at[d], r_d.at[d], h, r, 1 - c,
        ))
        if place:
            reduced[order[place - 1]] = reduce_block(order[place - 1], exchanges[order[place - 1]])
    reduce_block(0, exchanges[0])
    total = summed[0].astype(jnp.float32)
    for d in (1, 3, 2):
        reduced[d].wait_recv()
        total = total + got[d - 1].astype(jnp.float32)
    out_ref[mine, :] = (x_own[...].astype(jnp.float32) + 0.5 * total).astype(jnp.bfloat16)
    finish = go(remote(out_ref.at[mine], out_ref.at[mine], s_o.at[0], r_o.at[0], h, r, 1 - c))
    finish.wait_recv()
    for copy in started:
        copy.wait_send()


def interleave_kernel(width, gate_ref, up_ref, out_ref):
    even = width // 128 * 128
    for group in range(GROUPS):
        first = group * width
        gate, up = gate_ref[:, first:first + width], up_ref[:, first:first + width]
        for at in range(0, even, 128):
            out_ref[group, :, 2 * at:2 * at + 128] = gate[:, at:at + 128]
            out_ref[group, :, 2 * at + 128:2 * at + 256] = up[:, at:at + 128]
        if width > even:
            out_ref[group, :, 2 * even:] = jnp.concatenate([gate[:, even:], up[:, even:]], axis=1)


def layer(
    residual, queries, forget_gate_logits, projected_values, output_gate_logits, lower_bound_margin,
    extra_forget_logs, per_head_norm_gain, output_weight, feedforward_norm_gain, gate_weight, up_weight, down_weight,
):
    n_sp = lax.axis_size("sp")
    share, half = gate_weight.shape
    width = half // GROUPS
    padded = up_to(width, 128)
    length, model = residual.shape
    own = length // 2
    channels = queries.shape[1]
    message = channels + 16
    gu = pl.pallas_call(
        lambda *refs: interleave_kernel(width, *refs),
        out_shape=jax.ShapeDtypeStruct((GROUPS, share, 2 * width), jnp.bfloat16),
    )(gate_weight, up_weight)
    dn = down_weight.reshape(GROUPS, width, share)
    bf, f32 = jnp.bfloat16, jnp.float32
    dma = pltpu.SemaphoreType.DMA
    n_r = n_sp // GROUPS
    dims = (n_r, share, own, width, padded)
    vm = pl.BlockSpec(memory_space=pltpu.VMEM)
    hbm = pl.BlockSpec(memory_space=pl.ANY)
    return pl.pallas_call(
        lambda *refs: layer_kernel(dims, *refs),
        out_shape=jax.ShapeDtypeStruct((length, model), bf),
        in_specs=[hbm, hbm] + [vm] * 10,
        out_specs=vm,
        scratch_shapes=[
            pltpu.VMEM((model, 2 * width), bf),
            pltpu.VMEM((padded, model), bf),
            pltpu.VMEM((length, channels), f32),
            pltpu.VMEM((length, channels), bf),
            pltpu.VMEM((n_r, message, HD), bf),
            pltpu.VMEM((GROUPS, message, HD), bf),
            pltpu.VMEM((length, channels), bf),
            pltpu.VMEM((length, model), bf),
            pltpu.VMEM((own, model), bf),
            pltpu.VMEM((own, model), bf),
            pltpu.VMEM((GROUPS * length, model), bf),
            pltpu.VMEM((length, padded), bf),
            pltpu.VMEM((GROUPS, length, model), bf),
            pltpu.VMEM((GROUPS, own, model), bf),
            pltpu.VMEM((GROUPS, own, model), bf),
            pltpu.VMEM((GROUPS - 1, own, model), bf),
            dma((3, 2)), dma((3, 2)), dma((4, 3, 2)), dma((4, 3, 2)),
            dma((3,)), dma((3,)), dma((4,)), dma((4,)), dma((4,)), dma((4,)),
            dma((3,)), dma((3,)), dma((1,)), dma((1,)), dma((2,)),
            dma((3,)), dma((3,)), dma((3,)), dma((3,)), dma((1,)), dma((1,)),
        ],
        compiler_params=pltpu.CompilerParams(has_side_effects=True, vmem_limit_bytes=56 * 2**20),
    )(
        gu, dn, queries, forget_gate_logits, projected_values, output_gate_logits,
        lower_bound_margin.reshape(1, channels), extra_forget_logs, per_head_norm_gain.reshape(1, HD),
        output_weight, residual, feedforward_norm_gain.reshape(1, model),
    )


def fits(residual, queries, gate_weight):
    length, model = residual.shape
    share, half = gate_weight.shape
    return (
        lax.axis_size("sp") == 4 * GROUPS and lax.axis_size("tp") == 2 and share % 128 == 0
        and length % 128 == 0 and length <= 512 and half % (64 * GROUPS) == 0
        and queries.shape[1] <= 8 * HD and model % 256 == 0
    )


def local(
    residual,
    queries,
    forget_gate_logits,
    projected_values,
    output_gate_logits,
    lower_bound_margin,
    extra_forget_logs,
    per_head_norm_gain,
    output_weight,
    feedforward_norm_gain,
    gate_weight,
    up_weight,
    down_weight,
):
    if fits(residual, queries, gate_weight):
        return layer(
            residual, queries, forget_gate_logits, projected_values, output_gate_logits, lower_bound_margin,
            extra_forget_logs, per_head_norm_gain, output_weight, feedforward_norm_gain, gate_weight, up_weight, down_weight,
        )
    length = queries.shape[0]
    head_count = queries.shape[1] // HD
    state_increment = lower_bound_margin * jax.nn.sigmoid(-forget_gate_logits.astype(jnp.float32))
    retain_log_factor = jnp.log1p(-state_increment) + extra_forget_logs

    def to_blocks(source):
        return source.reshape(length // BLOCK, BLOCK, head_count, HD).transpose(0, 2, 1, 3)

    initial = (
        jnp.zeros((head_count, HD, HD), jnp.float32),
        jnp.zeros((head_count, HD), jnp.float32),
    )
    block_inputs = (
        to_blocks(queries.astype(jnp.float32)),
        to_blocks(state_increment),
        to_blocks(projected_values.astype(jnp.float32)),
        to_blocks(retain_log_factor),
    )
    (recurrent_state, decay_sum), (output_rows, rescaled_state) = lax.scan(
        block_update, initial, block_inputs
    )
    identity = (jnp.zeros_like(decay_sum), jnp.zeros_like(recurrent_state))
    incoming_state = carried_in_2((decay_sum, recurrent_state), "sp", join_states, identity)[1]
    output_rows = output_rows + jnp.einsum(
        "sjey,jyx->sjex", rescaled_state, incoming_state, precision=top_precision
    )
    mixed = output_rows.transpose(0, 2, 1, 3).reshape(length, head_count, HD)
    normed_heads = (
        mixed
        * lax.rsqrt(jnp.mean(mixed * mixed, axis=-1, keepdims=True) + eps)
        * per_head_norm_gain
    )
    gating = jax.nn.silu(output_gate_logits.astype(jnp.float32)).reshape(length, head_count, HD)
    gated = (normed_heads * gating).reshape(length, head_count * HD).astype(jnp.bfloat16)
    row_count = residual.shape[0] // lax.axis_size("tp")
    own_rows = lax.dynamic_slice_in_dim(residual, lax.axis_index("tp") * row_count, row_count, 0)
    rows_here = gated
    projected = lax.psum_scatter(
        jnp.dot(rows_here, output_weight, preferred_element_type=jnp.float32).astype(jnp.bfloat16),
        "tp",
        scatter_dimension=0,
        tiled=True,
    ).astype(jnp.float32)
    after_mixer = (own_rows.astype(jnp.float32) + projected).astype(jnp.bfloat16)
    widened = after_mixer.astype(jnp.float32)
    normed = (
        widened
        * lax.rsqrt(jnp.mean(widened * widened, axis=-1, keepdims=True) + eps)
        * feedforward_norm_gain
    ).astype(jnp.bfloat16)
    gate_full, up_full = (
        lax.all_gather(gate_weight, "sp", axis=0, tiled=True),
        lax.all_gather(up_weight, "sp", axis=0, tiled=True),
    )
    down_full = lax.all_gather(down_weight, "sp", axis=1, tiled=True)
    row_piece = lax.all_gather(normed, "tp", axis=0, tiled=True)
    gate_part = jnp.dot(row_piece, gate_full, preferred_element_type=jnp.float32)
    up_part = jnp.dot(row_piece, up_full, preferred_element_type=jnp.float32)
    hidden = (jax.nn.silu(gate_part) * up_part).astype(jnp.bfloat16)
    rows_here = hidden
    ffn_sum = lax.psum_scatter(
        jnp.dot(rows_here, down_full, preferred_element_type=jnp.float32).astype(jnp.bfloat16),
        "tp",
        scatter_dimension=0,
        tiled=True,
    ).astype(jnp.float32)
    finished = (after_mixer.astype(jnp.float32) + 0.5 * ffn_sum).astype(jnp.bfloat16)
    return lax.all_gather(finished, "tp", axis=0, tiled=True)


def solution(mesh):
    return jax.shard_map(
        local,
        mesh=mesh,
        in_specs=(
            P("sp", None),
            P("sp", "tp"),
            P("sp", "tp"),
            P("sp", "tp"),
            P("sp", "tp"),
            P("tp"),
            P("sp", "tp"),
            P(),
            P("tp", None),
            P(),
            P("sp", "tp"),
            P("sp", "tp"),
            P("tp", "sp"),
        ),
        out_specs=P("sp", None),
        check_vma=False,
    )
```

profile of v0, /device:TPU:1, one launch (start us, length us, event | category | flops | bytes accessed | tf_op | source)
XLA Modules:
  0.0 179.9 jit_solution(18033743067022472007)
XLA Ops:
  0.0 2.8 %shard_map.127.refs_0_ = bf16[4,128,1408]{2,1,0:T(8,128)(2,1)} custom-call(bf16[128,2816]{1,0:T(8,128)(2,1)} %refs_0_.1, bf16[128,2816]{1,0:T(8,128)(2,1)} %refs_1_.1), custom_call_target="tpu_custom_call" | custom-call | tf_op jit(solution)/shard_map/pallas_call | solution.py:365
  2.8 174.8 %shard_map.128 = bf16[256,2048]{1,0:T(8,128)(2,1)} custom-call(bf16[4,128,1408]{2,1,0:T(8,128)(2,1)} %shard_map.127.refs_0_, bf16[4,704,128]{2,1,0:T(8,128)(2,1)} %bitcast.4, bf16[256,512]{1,0:T(8,128)(2,1)} %refs_2_.1, bf16[256,512]{1,0:T(8,128)(2,1)} %refs_3_.1, bf16[256,512]{1,0:T(8,128)(2,1)} %refs_4_.1, bf16[256,512]{1,0:T(8,128)(2,1)} %refs_5_.1, ...), custom_call_target="tpu_custom_call" | custom-call | tf_op jit(solution)/shard_map/pallas_call | solution.py:376
  177.6 2.3 %copy.15 = bf16[256,2048]{1,0:T(8,128)(2,1)} copy(bf16[256,2048]{1,0:T(8,128)(2,1)} %shard_map.128) | data formatting | bytes 2097152
where the time goes:
time: 180 us
  Pallas kernels  178 us (99%)
  local copies, waits for them, and re-layouts  2.3 us (1%)
    pallas_call x1, Pallas kernels, layer(): pl.pallas_call(lambda *refs: layer_kernel(dims, *refs), out_shape=jax.Sha...  175 us

commit v1 on v0

v1 whole, which is shorter than its diff:
```python
import jax
import jax.numpy as jnp
from jax import lax
from jax.experimental import pallas as pl
from jax.experimental.pallas import tpu as pltpu
from jax.sharding import PartitionSpec as P

HD = 128
BLOCK = 64


eps = 1e-06
top_precision = lax.Precision.HIGHEST


def carried_in_2(value, axis, join, neutral):
    place = lax.axis_index(axis)
    gathered = jax.tree.map(
        lambda a, kind: lax.all_gather(a.astype(kind), axis), value, (jnp.bfloat16, jnp.bfloat16)
    )
    state = jax.tree.map(lambda a, e: jnp.zeros_like(a) + jnp.asarray(e, a.dtype), value, neutral)

    def one(turn, state):
        return join(
            state,
            jax.tree.map(
                lambda a, own: lax.dynamic_index_in_dim(a, turn, 0, False).astype(own.dtype),
                gathered,
                value,
            ),
        )

    return lax.fori_loop(0, place, one, state)


def block_update(carried_in, inputs):
    recurrent_state, offset = carried_in
    queries, state_increment, value_rows, retain_log_factor = inputs
    running_state = jnp.cumsum(retain_log_factor, axis=1)
    causal = jnp.tril(
        jnp.ones((retain_log_factor.shape[1], retain_log_factor.shape[1]), dtype=bool)
    )
    carried_over_state = jnp.einsum(
        "uqw,uwa->uqa", queries * jnp.exp(running_state), recurrent_state, precision=top_precision
    )
    spread = running_state[:, :, None, :] - running_state[:, None, :, :]
    weights = jnp.exp(jnp.where(causal[None, :, :, None], spread, -jnp.inf))
    scores = jnp.einsum(
        "htk,htsk,hsk->hts", queries, weights, state_increment, precision=top_precision
    )
    output_rows = carried_over_state + jnp.einsum(
        "hts,hsv->htv", scores, value_rows, precision=top_precision
    )
    final_state = running_state[:, -1:, :]
    updated_state = jnp.exp(final_state[:, 0, :])[:, :, None] * recurrent_state + jnp.einsum(
        "erb,erc->ebc",
        state_increment * jnp.exp(final_state - running_state),
        value_rows,
        precision=top_precision,
    )
    rescaled_state = queries * jnp.exp(running_state + offset[:, None, :])
    return ((updated_state, offset + final_state[:, 0, :]), (output_rows, rescaled_state))


def join_states(earlier, later):
    earlier_sum, earlier_memory = earlier
    later_sum, later_memory = later
    return (earlier_sum + later_sum, jnp.exp(later_sum)[:, :, None] * earlier_memory + later_memory)


MESH = pl.DeviceIdType.MESH
GROUPS = 4


def up_to(value, step):
    return -(-value // step) * step


def layer_kernel(
    dims, gate_hbm, up_hbm, dn_ref, q_hbm, f_hbm, v_hbm, og_hbm, extra_hbm, ow_hbm, res_hbm,
    margin_ref, head_gain_ref, ff_gain_ref, out_ref,
    gate_in, up_in, q_ref, f_ref, v_ref, og_ref, extra_ref, ow_ref, residual,
    gu_own, gu, dn, grown, q_grown, st_out, st_in, tot_out, tot_in, inc_out, inc,
    gated, proj, proj_got, x_own, rows_in, hid, part, peer_part, summed, xgot, pair, zgot,
    s_l, s_a, r_a, s_b, r_b, s_1, r_1, s_2, r_2, s_3, r_3, s_j, r_j, s_x, r_x, s_p, r_p,
    s_d, r_d, s_r, r_r, s_z, r_z, s_o, r_o,
):
    share, own, width, padded = dims
    me = lax.axis_index("sp")
    c = lax.axis_index("tp")
    z, r = me // 4, me % 4
    zh, zl, y, x = z // 2, z % 2, r // 2, r % 2
    inner = (zh + zl) % 2 == 1
    model = gu.shape[0]
    half = share // 2
    bf, f32 = jnp.bfloat16, jnp.float32

    def flip(value, d):
        return (value + d) % 2

    def place(o, dy=0):
        return (flip(zh, o // 4) * 2 + flip(zl, o // 2 % 2)) * 4 + flip(y, dy) * 2 + flip(x, o % 2)

    def group(o):
        return flip(x, o % 2) * 2 + flip(zl, o // 2 % 2)

    def beside(e):
        return flip(y, e // 2) * 2 + flip(x, e % 2)

    def remote(src, dst, send, recv, to, core):
        return pltpu.make_async_remote_copy(
            src_ref=src, dst_ref=dst, send_sem=send, recv_sem=recv, device_id=(to, core), device_id_type=MESH,
        )

    sent = []

    def go(copy):
        copy.start()
        sent.append(copy)
        return copy

    barrier = pltpu.get_barrier_semaphore()
    partners = [(place(o), c) for o in range(1, 8)] + [(place(0, 1), c), (place(1, 1), c), (me, 1 - c)]
    for partner in partners:
        pl.semaphore_signal(barrier, inc=1, device_id=partner, device_id_type=MESH)

    mine = pl.ds(pl.multiple_of(c * own, own), own)
    theirs = pl.ds(pl.multiple_of((1 - c) * own, own), own)
    loads = [
        pltpu.make_async_copy(src, dst, s_l.at[i])
        for i, (src, dst) in enumerate((
            (gate_hbm, gate_in), (up_hbm, up_in), (q_hbm, q_ref), (f_hbm, f_ref), (v_hbm, v_ref),
            (extra_hbm, extra_ref), (og_hbm, og_ref), (ow_hbm, ow_ref), (res_hbm.at[mine], residual),
            (dn_ref.at[group(0)], dn.at[pl.ds(0, width), pl.ds(pl.multiple_of(me * share, share), share)]),
        ))
    ]
    for load in loads:
        load.start()

    def region(owner, k):
        if k < 2:
            return gu.at[pl.ds(pl.multiple_of(owner * share + k * half, half), half)]
        return dn.at[pl.ds(0, width), pl.ds(pl.multiple_of(owner * share, share), share)]

    def origin(g, k):
        return gu_own.at[g, pl.ds(k * half, half)] if k < 2 else dn_ref.at[g]

    def direct(o, k):
        return remote(origin(group(o), k), region(me, k), s_a.at[o, k], r_a.at[o, k], place(o), c)

    def lend(o, k):
        block = region(place(o), k)
        return remote(origin(group(0), k) if o == 0 else block, block, s_b.at[o, k], r_b.at[o, k], place(0, 1), c)

    def send(*pieces):
        for o, k in pieces:
            direct(o, k).start()

    def relay(*pieces):
        for o, k in pieces:
            if o:
                direct(o, k).wait_recv()
            lend(o, k).start()

    loads[0].wait()
    loads[1].wait()
    even = width // 128 * 128
    for g in range(GROUPS):
        first = g * width
        gate, up = gate_in[:, first:first + width], up_in[:, first:first + width]
        for at in range(0, even, 128):
            gu_own[g, :, 2 * at:2 * at + 128] = gate[:, at:at + 128]
            gu_own[g, :, 2 * at + 128:2 * at + 256] = up[:, at:at + 128]
        if width > even:
            gu_own[g, :, 2 * even:] = jnp.concatenate([gate[:, even:], up[:, even:]], axis=1)
    gu[pl.ds(pl.multiple_of(me * share, share), share), :] = gu_own[group(0)]
    if padded > width:
        dn[pl.ds(width, padded - width), :] = jnp.zeros((padded - width, model), dn.dtype)

    pl.semaphore_wait(barrier, len(partners))

    @pl.when(inner)
    def _():
        send((4, 0), (6, 0))

    send((2, 0), (1, 0))
    relay((0, 0))

    length, channels = q_ref.shape
    heads = channels // HD
    span = 128
    ones = lambda n: lax.broadcasted_iota(jnp.int32, (n, n), 0) >= lax.broadcasted_iota(jnp.int32, (n, n), 1)
    lower = ones(length).astype(f32)
    causal = ones(span)
    over = lambda p, q, i, j: lax.dot_general(p, q, (((i,), (j,)), ((), ())), preferred_element_type=f32)

    def logs_tile(logs):
        high = logs.astype(bf)
        low = (logs - high.astype(f32)).astype(bf)
        return jnp.concatenate([jnp.broadcast_to(high, (8, HD)), jnp.broadcast_to(low, (8, HD))], axis=0)

    def part_of(ref, at):
        tile = ref[at, HD:HD + 16, :].astype(f32)
        return tile[0:1] + tile[8:9], ref[at, 0:HD, :].astype(f32)

    for i in range(2, 6):
        loads[i].wait()
    for n in range(heads):
        cols = slice(n * HD, (n + 1) * HD)
        inflow = margin_ref[:, cols] * jax.nn.sigmoid(-f_ref[:, cols].astype(f32))
        keep = jnp.log1p(-inflow) + extra_ref[:, cols]
        total_log = lax.dot_general(lower, keep, (((1,), (0,)), ((), ())), precision=top_precision, preferred_element_type=f32)
        q = q_ref[:, cols].astype(f32)
        q_grown[:, cols] = (q * jnp.exp(total_log)).astype(bf)
        state = None
        for start in range(0, length, span):
            rows = slice(start, start + span)
            a, qb, ub, vb = total_log[rows], q[rows], inflow[rows], v_ref[rows, cols]
            middle, end = a[span // 2 - 1:span // 2], a[span - 1:span]
            scores = over((qb * jnp.exp(a - middle)).astype(bf), (ub * jnp.exp(middle - a)).astype(bf), 1, 1)
            mixed = over(jnp.where(causal, scores, 0.0).astype(bf), vb, 1, 0)
            added = over(vb, (ub * jnp.exp(end - a)).astype(bf), 0, 0)
            if state is None:
                state = added
            else:
                mixed = mixed + over((qb * jnp.exp(a - base)).astype(bf), state.astype(bf), 1, 1)
                state = state * jnp.exp(end - base) + added
            grown[rows, cols] = mixed
            base = end
        st_out[n, 0:HD, :] = state.astype(bf)
        st_out[n, HD:HD + 16, :] = logs_tile(base)

    to_head = [
        go(remote(st_out.at[beside(e)], st_in.at[r], s_1.at[e - 1], r_1.at[e - 1], z * 4 + beside(e), c)) for e in (3, 1, 2)
    ]
    st_in[r] = st_out[r]
    send((1, 1))
    relay((0, 1), (0, 2))
    for copy in to_head:
        copy.wait_recv()
    whole, whole_log, before = jnp.zeros((HD, HD), f32), jnp.zeros((1, HD), f32), []
    for at in range(4):
        logs, state = part_of(st_in, at)
        before.append((whole_log, whole))
        whole = whole * jnp.exp(logs) + state
        whole_log = whole_log + logs
    tot_out[0, 0:HD, :] = whole.astype(bf)
    tot_out[0, HD:HD + 16, :] = logs_tile(whole_log)
    along = [go(remote(tot_out.at[0], tot_in.at[z], s_2.at[d - 1], r_2.at[d - 1], place(2 * d), c)) for d in (2, 3, 1)]

    @pl.when(inner)
    def _():
        send((4, 1), (6, 1), (4, 2))

    @pl.when(jnp.logical_not(inner))
    def _():
        send((4, 0), (6, 0), (4, 1))

    send((1, 2))
    for copy in along:
        copy.wait_recv()
    state = jnp.zeros((HD, HD), f32)
    for at in range(3):
        logs, later = part_of(tot_in, at)
        state = jnp.where(at < z, state * jnp.exp(logs) + later, state)
    for at in range(4):
        early_log, early = before[at]
        inc_out[at] = (state * jnp.exp(early_log) + early).astype(bf)
    to_rows = [
        go(remote(inc_out.at[beside(e)], inc.at[r], s_3.at[e - 1], r_3.at[e - 1], z * 4 + beside(e), c)) for e in (3, 1, 2)
    ]
    inc[r] = inc_out[r]
    send((5, 0), (7, 0))
    relay((1, 0), (2, 0))
    for i in range(6, 9):
        loads[i].wait()
    for copy in to_rows:
        copy.wait_recv()
    for n in range(heads):
        cols = slice(n * HD, (n + 1) * HD)
        mixed = grown[:, cols] + over(q_grown[:, cols], inc[n], 1, 1)
        scale = lax.rsqrt(jnp.mean(mixed * mixed, axis=-1, keepdims=True) + eps)
        gate = og_ref[:, cols].astype(f32)
        gated[:, cols] = (mixed * scale * head_gain_ref[...] * (gate * jax.nn.sigmoid(gate))).astype(bf)

    def project(j, carry):
        at = pl.multiple_of(j * 256, 256)
        proj[:, pl.ds(at, 256)] = jnp.dot(
            gated[...], ow_ref[:, pl.ds(at, 256)], preferred_element_type=f32
        ).astype(bf)
        return carry

    lax.fori_loop(0, model // 256, project, 0)
    joined = go(remote(proj.at[theirs], proj_got, s_j.at[0], r_j.at[0], me, 1 - c))
    relay((1, 1))
    joined.wait_recv()
    after = (residual[...].astype(f32) + (proj[mine, :].astype(f32) + proj_got[...].astype(f32))).astype(bf)
    x_own[...] = after
    wide = after.astype(f32)
    normed = wide * lax.rsqrt(jnp.mean(wide * wide, axis=-1, keepdims=True) + eps) * ff_gain_ref[...]

    def token_rows(o):
        return pl.ds(pl.multiple_of((c * GROUPS + group(o)) * own, own), own)

    rows_in[token_rows(0), :] = normed.astype(bf)

    def rows_to(o, i, to, core):
        block = rows_in.at[token_rows(o)]
        return go(remote(block, block, s_x.at[i], r_x.at[i], to, core))

    def rows_over(o):
        block = rows_in.at[token_rows(o)]
        return go(remote(block, block, s_p.at[o], r_p.at[o], me, 1 - c))

    to_x, to_z = rows_to(0, 0, place(1), c), rows_to(0, 1, place(2), c)
    peers = [rows_over(0)]

    @pl.when(inner)
    def _():
        send((2, 1), (6, 2), (2, 2))

    @pl.when(jnp.logical_not(inner))
    def _():
        send((6, 1), (2, 1), (4, 2), (6, 2), (2, 2))

    send((5, 1), (7, 1))
    relay((4, 0), (6, 0), (4, 1))
    to_z.wait_recv()
    to_x2 = rows_to(2, 2, place(1), c)
    peers.append(rows_over(2))
    send((3, 0), (3, 1), (5, 2), (7, 2), (3, 2))
    to_x.wait_recv()
    peers.append(rows_over(1))
    relay((1, 2), (6, 1), (2, 1), (5, 0), (7, 0), (5, 1), (7, 1))
    to_x2.wait_recv()
    peers.append(rows_over(3))
    relay((3, 0), (3, 1))
    relay((2, 2), (4, 2))
    for copy in peers:
        copy.wait_recv()
    for o in range(8):
        for k in (0, 1):
            lend(o, k).wait_recv()

    block_rows = 4 * own

    def gate_up(m):
        rows = pl.ds(m * block_rows, block_rows)

        def step(j, carry):
            at = pl.multiple_of(j * 256, 256)
            both = jnp.dot(rows_in[rows, :], gu[:, pl.ds(at, 256)], preferred_element_type=f32)
            gate, up = both[:, :128], both[:, 128:]
            hid[rows, pl.ds(pl.multiple_of(j * 128, 128), 128)] = (gate * jax.nn.sigmoid(gate) * up).astype(bf)
            return carry

        lax.fori_loop(0, width // 128, step, 0)
        if width % 128:
            both = jnp.dot(rows_in[rows, :], gu[:, 2 * even:], preferred_element_type=f32)
            hid[rows, even:] = (both * jax.nn.sigmoid(both) * pltpu.roll(both, 64, 1)).astype(bf)

    gate_up(0)
    relay((6, 2))
    gate_up(1)
    loads[9].wait()

    tile = 2 * share
    my_rows = pl.ds(pl.multiple_of(c * block_rows, block_rows), block_rows)
    their_rows = pl.ds(pl.multiple_of((1 - c) * block_rows, block_rows), block_rows)
    row_pair = pl.ds(pl.multiple_of(x * 2 * own, own), 2 * own)
    other_pair = pl.ds(pl.multiple_of((1 - x) * 2 * own, own), 2 * own)
    row_own = pl.ds(pl.multiple_of(zl * own, own), own)
    row_other = pl.ds(pl.multiple_of((1 - zl) * own, own), own)

    def columns(k):
        at = (flip(zh, k // 4) * 2 + k // 2 % 2) * 4 + flip(y, k % 2) * 2
        return pl.ds(pl.multiple_of(at * share, tile), tile)

    def swap(k):
        return remote(part.at[k, their_rows], peer_part.at[k], s_d.at[k], r_d.at[k], me, 1 - c)

    def across_x(k):
        return remote(summed.at[k, other_pair], xgot.at[k], s_r.at[k], r_r.at[k], place(1), c)

    def across_z(k):
        return remote(pair.at[k, row_other], zgot.at[k], s_z.at[k], r_z.at[k], place(2), c)

    def finish(k):
        block = out_ref.at[mine, columns(k)]
        return remote(block, block, s_o.at[k], r_o.at[k], me, 1 - c)

    def down(k):
        for m in range(2):
            rows = pl.ds(m * block_rows, block_rows)
            part[k, rows, :] = jnp.dot(hid[rows, :], dn[:, columns(k)], preferred_element_type=f32).astype(bf)
        swap(k).start()

    def stage_1(k):
        swap(k).wait_recv()
        summed[k] = (part[k, my_rows, :].astype(f32) + peer_part[k].astype(f32)).astype(bf)
        across_x(k).start()

    def stage_2(k):
        across_x(k).wait_recv()
        pair[k] = (summed[k, row_pair, :].astype(f32) + xgot[k].astype(f32)).astype(bf)
        across_z(k).start()

    def stage_3(k):
        across_z(k).wait_recv()
        total = pair[k, row_own, :].astype(f32) + zgot[k].astype(f32)
        out_ref[mine, columns(k)] = (x_own[:, columns(k)].astype(f32) + 0.5 * total).astype(bf)
        finish(k).start()

    order = (0, 2, 1, 3, 4, 6, 5, 7)
    for turn in range(len(order) + 3):
        if turn == 0:
            relay((3, 2))
        if turn == 1:
            relay((5, 2))
        if turn == 2:
            for o in range(4):
                lend(o, 2).wait_recv()
            relay((7, 2))
        if turn == 6:
            for o in range(4, 8):
                lend(o, 2).wait_recv()
        if turn < len(order):
            down(order[turn])
        if 1 <= turn <= len(order):
            stage_1(order[turn - 1])
        if 2 <= turn <= len(order) + 1:
            stage_2(order[turn - 2])
        if turn >= 3:
            stage_3(order[turn - 3])
    for k in range(8):
        finish(k).wait_recv()
    for copy in sent:
        copy.wait_send()
    for o in range(8):
        for k in range(3):
            if o:
                direct(o, k).wait_send()
            lend(o, k).wait_send()
    for k in range(8):
        for copy in (swap(k), across_x(k), across_z(k), finish(k)):
            copy.wait_send()


def layer(
    residual, queries, forget_gate_logits, projected_values, output_gate_logits, lower_bound_margin,
    extra_forget_logs, per_head_norm_gain, output_weight, feedforward_norm_gain, gate_weight, up_weight, down_weight,
):
    share, half = gate_weight.shape
    width = half // GROUPS
    padded = up_to(width, 128)
    length, model = residual.shape
    own = length // 2
    channels = queries.shape[1]
    dn = down_weight.reshape(GROUPS, width, share)
    bf, f32 = jnp.bfloat16, jnp.float32
    dma = pltpu.SemaphoreType.DMA
    dims = (share, own, width, padded)
    vm = pl.BlockSpec(memory_space=pltpu.VMEM)
    hbm = pl.BlockSpec(memory_space=pltpu.HBM)
    message = HD + 16
    tile = 2 * share
    chunks = model // tile
    return pl.pallas_call(
        lambda *refs: layer_kernel(dims, *refs),
        out_shape=jax.ShapeDtypeStruct((length, model), bf),
        in_specs=[hbm] * 10 + [vm] * 3,
        out_specs=vm,
        scratch_shapes=[
            pltpu.VMEM((share, half), bf),
            pltpu.VMEM((share, half), bf),
            pltpu.VMEM((length, channels), bf),
            pltpu.VMEM((length, channels), bf),
            pltpu.VMEM((length, channels), bf),
            pltpu.VMEM((length, channels), bf),
            pltpu.VMEM((length, channels), f32),
            pltpu.VMEM((channels, model), bf),
            pltpu.VMEM((own, model), bf),
            pltpu.VMEM((GROUPS, share, 2 * width), bf),
            pltpu.VMEM((model, 2 * width), bf),
            pltpu.VMEM((padded, model), bf),
            pltpu.VMEM((length, channels), f32),
            pltpu.VMEM((length, channels), bf),
            pltpu.VMEM((4, message, HD), bf),
            pltpu.VMEM((4, message, HD), bf),
            pltpu.VMEM((1, message, HD), bf),
            pltpu.VMEM((4, message, HD), bf),
            pltpu.VMEM((4, HD, HD), bf),
            pltpu.VMEM((4, HD, HD), bf),
            pltpu.VMEM((length, channels), bf),
            pltpu.VMEM((length, model), bf),
            pltpu.VMEM((own, model), bf),
            pltpu.VMEM((own, model), bf),
            pltpu.VMEM((GROUPS * length, model), bf),
            pltpu.VMEM((GROUPS * length, padded), bf),
            pltpu.VMEM((chunks, GROUPS * length, tile), bf),
            pltpu.VMEM((chunks, GROUPS * own, tile), bf),
            pltpu.VMEM((chunks, GROUPS * own, tile), bf),
            pltpu.VMEM((chunks, 2 * own, tile), bf),
            pltpu.VMEM((chunks, 2 * own, tile), bf),
            pltpu.VMEM((chunks, own, tile), bf),
            dma((10,)), dma((8, 3)), dma((8, 3)), dma((8, 3)), dma((8, 3)),
            dma((3,)), dma((3,)), dma((3,)), dma((3,)), dma((3,)), dma((3,)), dma((1,)), dma((1,)),
            dma((3,)), dma((3,)), dma((4,)), dma((4,)),
            dma((chunks,)), dma((chunks,)), dma((chunks,)), dma((chunks,)), dma((chunks,)), dma((chunks,)),
            dma((chunks,)), dma((chunks,)),
        ],
        compiler_params=pltpu.CompilerParams(
            has_side_effects=True, collective_id=0, vmem_limit_bytes=60 * 2**20
        ),
    )(
        gate_weight, up_weight, dn, queries, forget_gate_logits, projected_values, output_gate_logits,
        extra_forget_logs, output_weight, residual,
        lower_bound_margin.reshape(1, channels), per_head_norm_gain.reshape(1, HD),
        feedforward_norm_gain.reshape(1, model),
    )


def fits(residual, queries, gate_weight):
    length, model = residual.shape
    share, half = gate_weight.shape
    return (
        lax.axis_size("sp") == 4 * GROUPS and lax.axis_size("tp") == 2 and share == HD
        and length % 256 == 0 and length <= 512 and half % (64 * GROUPS) == 0
        and queries.shape[1] == GROUPS * HD and model == 4 * GROUPS * share
    )


def local(
    residual,
    queries,
    forget_gate_logits,
    projected_values,
    output_gate_logits,
    lower_bound_margin,
    extra_forget_logs,
    per_head_norm_gain,
    output_weight,
    feedforward_norm_gain,
    gate_weight,
    up_weight,
    down_weight,
):
    if fits(residual, queries, gate_weight):
        return layer(
            residual, queries, forget_gate_logits, projected_values, output_gate_logits, lower_bound_margin,
            extra_forget_logs, per_head_norm_gain, output_weight, feedforward_norm_gain, gate_weight, up_weight, down_weight,
        )
    length = queries.shape[0]
    head_count = queries.shape[1] // HD
    state_increment = lower_bound_margin * jax.nn.sigmoid(-forget_gate_logits.astype(jnp.float32))
    retain_log_factor = jnp.log1p(-state_increment) + extra_forget_logs

    def to_blocks(source):
        return source.reshape(length // BLOCK, BLOCK, head_count, HD).transpose(0, 2, 1, 3)

    initial = (
        jnp.zeros((head_count, HD, HD), jnp.float32),
        jnp.zeros((head_count, HD), jnp.float32),
    )
    block_inputs = (
        to_blocks(queries.astype(jnp.float32)),
        to_blocks(state_increment),
        to_blocks(projected_values.astype(jnp.float32)),
        to_blocks(retain_log_factor),
    )
    (recurrent_state, decay_sum), (output_rows, rescaled_state) = lax.scan(
        block_update, initial, block_inputs
    )
    identity = (jnp.zeros_like(decay_sum), jnp.zeros_like(recurrent_state))
    incoming_state = carried_in_2((decay_sum, recurrent_state), "sp", join_states, identity)[1]
    output_rows = output_rows + jnp.einsum(
        "sjey,jyx->sjex", rescaled_state, incoming_state, precision=top_precision
    )
    mixed = output_rows.transpose(0, 2, 1, 3).reshape(length, head_count, HD)
    normed_heads = (
        mixed
        * lax.rsqrt(jnp.mean(mixed * mixed, axis=-1, keepdims=True) + eps)
        * per_head_norm_gain
    )
    gating = jax.nn.silu(output_gate_logits.astype(jnp.float32)).reshape(length, head_count, HD)
    gated = (normed_heads * gating).reshape(length, head_count * HD).astype(jnp.bfloat16)
    row_count = residual.shape[0] // lax.axis_size("tp")
    own_rows = lax.dynamic_slice_in_dim(residual, lax.axis_index("tp") * row_count, row_count, 0)
    rows_here = gated
    projected = lax.psum_scatter(
        jnp.dot(rows_here, output_weight, preferred_element_type=jnp.float32).astype(jnp.bfloat16),
        "tp",
        scatter_dimension=0,
        tiled=True,
    ).astype(jnp.float32)
    after_mixer = (own_rows.astype(jnp.float32) + projected).astype(jnp.bfloat16)
    widened = after_mixer.astype(jnp.float32)
    normed = (
        widened
        * lax.rsqrt(jnp.mean(widened * widened, axis=-1, keepdims=True) + eps)
        * feedforward_norm_gain
    ).astype(jnp.bfloat16)
    gate_full, up_full = (
        lax.all_gather(gate_weight, "sp", axis=0, tiled=True),
        lax.all_gather(up_weight, "sp", axis=0, tiled=True),
    )
    down_full = lax.all_gather(down_weight, "sp", axis=1, tiled=True)
    row_piece = lax.all_gather(normed, "tp", axis=0, tiled=True)
    gate_part = jnp.dot(row_piece, gate_full, preferred_element_type=jnp.float32)
    up_part = jnp.dot(row_piece, up_full, preferred_element_type=jnp.float32)
    hidden = (jax.nn.silu(gate_part) * up_part).astype(jnp.bfloat16)
    rows_here = hidden
    ffn_sum = lax.psum_scatter(
        jnp.dot(rows_here, down_full, preferred_element_type=jnp.float32).astype(jnp.bfloat16),
        "tp",
        scatter_dimension=0,
        tiled=True,
    ).astype(jnp.float32)
    finished = (after_mixer.astype(jnp.float32) + 0.5 * ffn_sum).astype(jnp.bfloat16)
    return lax.all_gather(finished, "tp", axis=0, tiled=True)


def solution(mesh):
    return jax.shard_map(
        local,
        mesh=mesh,
        in_specs=(
            P("sp", None),
            P("sp", "tp"),
            P("sp", "tp"),
            P("sp", "tp"),
            P("sp", "tp"),
            P("tp"),
            P("sp", "tp"),
            P(),
            P("tp", None),
            P(),
            P("sp", "tp"),
            P("sp", "tp"),
            P("tp", "sp"),
        ),
        out_specs=P("sp", None),
        check_vma=False,
    )
```

time: 180 us -> 168 us (0.933)
  Pallas kernels: 178 us -> 165 us
    pallas_call x1, Pallas kernels: 175 us -> 165 us  [layer(): pl.pallas_call(lambda *refs: layer_kernel(dims, *refs), out_shape=jax.Sha...]
    pallas_call x1 -> x0, Pallas kernels: 2.8 us -> none  [layer(): pl.pallas_call(lambda *refs: interleave_kernel(width, *refs), out_shape=j...]
where the time goes in v1:
time: 168 us
  Pallas kernels  165 us (98%)
  local copies, waits for them, and re-layouts  2.3 us (1%)
    pallas_call x1, Pallas kernels, layer(): pl.pallas_call(lambda *refs: layer_kernel(dims, *refs), out_shape=jax.Sha...  165 us

profile of v1, /device:TPU:1, one launch (start us, length us, event | category | flops | bytes accessed | tf_op | source)
XLA Modules:
  0.0 167.6 jit_solution(13100223944909353474)
XLA Ops:
  0.0 165.2 %shard_map.127 = bf16[256,2048]{1,0:T(8,128)(2,1)} custom-call(bf16[128,2816]{1,0:T(8,128)(2,1)} %refs_0_.1, bf16[128,2816]{1,0:T(8,128)(2,1)} %refs_1_.1, bf16[4,704,128]{2,1,0:T(8,128)(2,1)} %bitcast.4, bf16[256,512]{1,0:T(8,128)(2,1)} %refs_3_.1, bf16[256,512]{1,0:T(8,128)(2,1)} %refs_4_.1, bf16[256,512]{1,0:T(8,128)(2,1)} %refs_5_.1, ...), custom_call_target="tpu_custom_call" | custom-call | tf_op jit(solution)/shard_map/pallas_call | solution.py:468
  165.3 2.3 %copy.15 = bf16[256,2048]{1,0:T(8,128)(2,1)} copy(bf16[256,2048]{1,0:T(8,128)(2,1)} %shard_map.127) | data formatting | bytes 2097152

commit v2 on v1

--- a/solution.py
+++ b/solution.py
@@ -80,9 +80,9 @@
     dims, gate_hbm, up_hbm, dn_ref, q_hbm, f_hbm, v_hbm, og_hbm, extra_hbm, ow_hbm, res_hbm,
     margin_ref, head_gain_ref, ff_gain_ref, out_ref,
     gate_in, up_in, q_ref, f_ref, v_ref, og_ref, extra_ref, ow_ref, residual,
-    gu_own, gu, dn, grown, q_grown, st_out, st_in, tot_out, tot_in, inc_out, inc,
+    gu_own, gu, dn, gu_pass, dn_pass, grown, q_grown, st_out, st_in, tot_out, tot_in, inc_out, inc,
     gated, proj, proj_got, x_own, rows_in, hid, part, peer_part, summed, xgot, pair, zgot,
-    s_l, s_a, r_a, s_b, r_b, s_1, r_1, s_2, r_2, s_3, r_3, s_j, r_j, s_x, r_x, s_p, r_p,
+    s_l, s_a, r_a, s_b, r_b, s_g, r_g, s_1, r_1, s_2, r_2, s_3, r_3, s_j, r_j, s_x, r_x, s_p, r_p,
     s_d, r_d, s_r, r_r, s_z, r_z, s_o, r_o,
 ):
     share, own, width, padded = dims
@@ -145,8 +145,26 @@
     def origin(g, k):
         return gu_own.at[g, pl.ds(k * half, half)] if k < 2 else dn_ref.at[g]
 
+    def passing(k):
+        return gu_pass.at[pl.ds(k * half, half)] if k < 2 else dn_pass
+
     def direct(o, k):
+        if o in (3, 5, 7):
+            block = region(place(1), k)
+            return remote(block if o == 5 else passing(k), block, s_a.at[o, k], r_a.at[o, k], place(o - 1), c)
         return remote(origin(group(o), k), region(me, k), s_a.at[o, k], r_a.at[o, k], place(o), c)
+
+    passed = {}
+
+    def pass_over(k):
+        passed[k] = go(remote(origin(group(3), k), passing(k), s_g.at[k], r_g.at[k], place(1), c))
+
+    def take(k):
+        direct(1, k).wait_recv()
+
+    def take_passed(k):
+        copy = passed[k]
+        copy.wait_recv()
 
     def lend(o, k):
         block = region(place(o), k)
@@ -158,10 +176,25 @@
 
     def relay(*pieces):
         for o, k in pieces:
-            if o:
+            if o > 1:
                 direct(o, k).wait_recv()
             lend(o, k).start()
 
+    def by_place(act, outer=(), between=()):
+        @pl.when(inner)
+        def _():
+            act(*between)
+
+        @pl.when(jnp.logical_not(inner))
+        def _():
+            act(*outer)
+
+    if padded > width:
+        dn[pl.ds(width, padded - width), :] = jnp.zeros((padded - width, model), dn.dtype)
+    pl.semaphore_wait(barrier, len(partners))
+    by_place(send, ((2, 2),), ((6, 2), (2, 2)))
+    send((1, 2))
+    relay((0, 2))
     loads[0].wait()
     loads[1].wait()
     even = width // 128 * 128
@@ -174,17 +207,7 @@
         if width > even:
             gu_own[g, :, 2 * even:] = jnp.concatenate([gate[:, even:], up[:, even:]], axis=1)
     gu[pl.ds(pl.multiple_of(me * share, share), share), :] = gu_own[group(0)]
-    if padded > width:
-        dn[pl.ds(width, padded - width), :] = jnp.zeros((padded - width, model), dn.dtype)
-
-    pl.semaphore_wait(barrier, len(partners))
-
-    @pl.when(inner)
-    def _():
-        send((4, 0), (6, 0))
-
-    send((2, 0), (1, 0))
-    relay((0, 0))
+    by_place(send, ((2, 0),), ((4, 0), (2, 0)))
 
     length, channels = q_ref.shape
     heads = channels // HD
@@ -234,8 +257,10 @@
         go(remote(st_out.at[beside(e)], st_in.at[r], s_1.at[e - 1], r_1.at[e - 1], z * 4 + beside(e), c)) for e in (3, 1, 2)
     ]
     st_in[r] = st_out[r]
-    send((1, 1))
-    relay((0, 1), (0, 2))
+    send((1, 0))
+    pass_over(0)
+    by_place(send, (), ((4, 1),))
+    relay((0, 0), (0, 1))
     for copy in to_head:
         copy.wait_recv()
     whole, whole_log, before = jnp.zeros((HD, HD), f32), jnp.zeros((1, HD), f32), []
@@ -246,23 +271,28 @@
         whole_log = whole_log + logs
     tot_out[0, 0:HD, :] = whole.astype(bf)
     tot_out[0, HD:HD + 16, :] = logs_tile(whole_log)
-    along = [go(remote(tot_out.at[0], tot_in.at[z], s_2.at[d - 1], r_2.at[d - 1], place(2 * d), c)) for d in (2, 3, 1)]
-
-    @pl.when(inner)
-    def _():
-        send((4, 1), (6, 1), (4, 2))
-
-    @pl.when(jnp.logical_not(inner))
-    def _():
-        send((4, 0), (6, 0), (4, 1))
-
-    send((1, 2))
-    for copy in along:
-        copy.wait_recv()
+
+    def total_to(d):
+        return remote(tot_out.at[0], tot_in.at[z], s_2.at[d - 1], r_2.at[d - 1], place(2 * d), c)
+
+    later = {1: zl == 0, 2: zh == 0, 3: zh == 0}
+    for d in (2, 3, 1):
+        @pl.when(later[d])
+        def _():
+            total_to(d).start()
+
+    by_place(send, ((2, 1),), ((6, 0), (2, 1)))
+    take(2)
+    relay((1, 2))
+    for d in (2, 3, 1):
+        @pl.when(jnp.logical_not(later[d]))
+        def _():
+            total_to(d).wait_recv()
+
     state = jnp.zeros((HD, HD), f32)
     for at in range(3):
-        logs, later = part_of(tot_in, at)
-        state = jnp.where(at < z, state * jnp.exp(logs) + later, state)
+        logs, added = part_of(tot_in, at)
+        state = jnp.where(at < z, state * jnp.exp(logs) + added, state)
     for at in range(4):
         early_log, early = before[at]
         inc_out[at] = (state * jnp.exp(early_log) + early).astype(bf)
@@ -270,12 +300,20 @@
         go(remote(inc_out.at[beside(e)], inc.at[r], s_3.at[e - 1], r_3.at[e - 1], z * 4 + beside(e), c)) for e in (3, 1, 2)
     ]
     inc[r] = inc_out[r]
-    send((5, 0), (7, 0))
-    relay((1, 0), (2, 0))
+    send((1, 1))
+    pass_over(1)
+    take(0)
+    by_place(send, ((4, 0),), ((5, 0), (6, 1)))
+    relay((1, 0))
     for i in range(6, 9):
         loads[i].wait()
     for copy in to_rows:
         copy.wait_recv()
+    pass_over(2)
+    take_passed(0)
+    take(1)
+    by_place(send, ((3, 0), (6, 0)), ((5, 1), (3, 0), (4, 2), (7, 0)))
+    relay((2, 0), (2, 2))
     for n in range(heads):
         cols = slice(n * HD, (n + 1) * HD)
         mixed = grown[:, cols] + over(q_grown[:, cols], inc[n], 1, 1)
@@ -283,16 +321,19 @@
         gate = og_ref[:, cols].astype(f32)
         gated[:, cols] = (mixed * scale * head_gain_ref[...] * (gate * jax.nn.sigmoid(gate))).astype(bf)
 
-    def project(j, carry):
-        at = pl.multiple_of(j * 256, 256)
-        proj[:, pl.ds(at, 256)] = jnp.dot(
-            gated[...], ow_ref[:, pl.ds(at, 256)], preferred_element_type=f32
-        ).astype(bf)
-        return carry
-
-    lax.fori_loop(0, model // 256, project, 0)
+    def project(rows):
+        def step(j, carry):
+            at = pl.multiple_of(j * 256, 256)
+            proj[rows, pl.ds(at, 256)] = jnp.dot(
+                gated[rows, :], ow_ref[:, pl.ds(at, 256)], preferred_element_type=f32
+            ).astype(bf)
+            return carry
+
+        lax.fori_loop(0, model // 256, step, 0)
+
+    project(theirs)
     joined = go(remote(proj.at[theirs], proj_got, s_j.at[0], r_j.at[0], me, 1 - c))
-    relay((1, 1))
+    project(mine)
     joined.wait_recv()
     after = (residual[...].astype(f32) + (proj[mine, :].astype(f32) + proj_got[...].astype(f32))).astype(bf)
     x_own[...] = after
@@ -315,27 +356,28 @@
     to_x, to_z = rows_to(0, 0, place(1), c), rows_to(0, 1, place(2), c)
     peers = [rows_over(0)]
 
-    @pl.when(inner)
-    def _():
-        send((2, 1), (6, 2), (2, 2))
-
-    @pl.when(jnp.logical_not(inner))
-    def _():
-        send((6, 1), (2, 1), (4, 2), (6, 2), (2, 2))
-
-    send((5, 1), (7, 1))
-    relay((4, 0), (6, 0), (4, 1))
+    take_passed(1)
+    by_place(send, (), ((7, 1),))
+    relay((1, 1), (2, 1))
+    by_place(relay, ((4, 0), (4, 1)), ((6, 0), (6, 1)))
+    take_passed(2)
+    by_place(send, (), ((7, 2),))
     to_z.wait_recv()
     to_x2 = rows_to(2, 2, place(1), c)
     peers.append(rows_over(2))
-    send((3, 0), (3, 1), (5, 2), (7, 2), (3, 2))
+    by_place(
+        send, ((7, 0), (4, 1), (6, 1), (5, 0), (7, 1), (5, 1), (3, 1), (3, 2), (4, 2), (6, 2), (5, 2), (7, 2)),
+        ((3, 1), (3, 2), (5, 2)),
+    )
     to_x.wait_recv()
     peers.append(rows_over(1))
-    relay((1, 2), (6, 1), (2, 1), (5, 0), (7, 0), (5, 1), (7, 1))
+    by_place(relay, ((5, 0), (6, 0)), ((4, 0), (7, 0), (3, 0)))
     to_x2.wait_recv()
     peers.append(rows_over(3))
-    relay((3, 0), (3, 1))
-    relay((2, 2), (4, 2))
+    by_place(relay, ((5, 1), (3, 0)), ((7, 1), (6, 2)))
+    by_place(relay, ((7, 0), (3, 1)), ((4, 1), (7, 2)))
+    by_place(relay, ((6, 1), (7, 1)), ((5, 0), (5, 1), (3, 1)))
+    by_place(relay, ((4, 2), (3, 2)), ())
     for copy in peers:
         copy.wait_recv()
     for o in range(8):
@@ -360,17 +402,15 @@
             hid[rows, even:] = (both * jax.nn.sigmoid(both) * pltpu.roll(both, 64, 1)).astype(bf)
 
     gate_up(0)
-    relay((6, 2))
+    by_place(relay, ((5, 2),), ((3, 2),))
     gate_up(1)
     loads[9].wait()
 
     tile = 2 * share
     my_rows = pl.ds(pl.multiple_of(c * block_rows, block_rows), block_rows)
     their_rows = pl.ds(pl.multiple_of((1 - c) * block_rows, block_rows), block_rows)
-    row_pair = pl.ds(pl.multiple_of(x * 2 * own, own), 2 * own)
-    other_pair = pl.ds(pl.multiple_of((1 - x) * 2 * own, own), 2 * own)
-    row_own = pl.ds(pl.multiple_of(zl * own, own), own)
-    row_other = pl.ds(pl.multiple_of((1 - zl) * own, own), own)
+    def group_rows(xx, zz):
+        return pl.ds(pl.multiple_of((xx * 2 + zz) * own, own), own)
 
     def columns(k):
         at = (flip(zh, k // 4) * 2 + k // 2 % 2) * 4 + flip(y, k % 2) * 2
@@ -379,11 +419,20 @@
     def swap(k):
         return remote(part.at[k, their_rows], peer_part.at[k], s_d.at[k], r_d.at[k], me, 1 - c)
 
-    def across_x(k):
-        return remote(summed.at[k, other_pair], xgot.at[k], s_r.at[k], r_r.at[k], place(1), c)
-
-    def across_z(k):
-        return remote(pair.at[k, row_other], zgot.at[k], s_z.at[k], r_z.at[k], place(2), c)
+    def x_first(k):
+        return k in (0, 1, 4, 5)
+
+    def first_hop(k, i):
+        if x_first(k):
+            rows, to = group_rows(1 - x, i), place(1)
+        else:
+            rows, to = group_rows(i, 1 - zl), place(2)
+        return remote(summed.at[k, rows], xgot.at[k, i], s_r.at[k, i], r_r.at[k, i], to, c)
+
+    def second_hop(k):
+        if x_first(k):
+            return remote(pair.at[k, 1 - zl], zgot.at[k], s_z.at[k], r_z.at[k], place(2), c)
+        return remote(pair.at[k, 1 - x], zgot.at[k], s_z.at[k], r_z.at[k], place(1), c)
 
     def finish(k):
         block = out_ref.at[mine, columns(k)]
@@ -398,29 +447,31 @@
     def stage_1(k):
         swap(k).wait_recv()
         summed[k] = (part[k, my_rows, :].astype(f32) + peer_part[k].astype(f32)).astype(bf)
-        across_x(k).start()
+        for i in range(2):
+            first_hop(k, i).start()
 
     def stage_2(k):
-        across_x(k).wait_recv()
-        pair[k] = (summed[k, row_pair, :].astype(f32) + xgot[k].astype(f32)).astype(bf)
-        across_z(k).start()
+        for i in range(2):
+            first_hop(k, i).wait_recv()
+            rows = group_rows(x, i) if x_first(k) else group_rows(i, zl)
+            pair[k, i] = (summed[k, rows, :].astype(f32) + xgot[k, i].astype(f32)).astype(bf)
+        second_hop(k).start()
 
     def stage_3(k):
-        across_z(k).wait_recv()
-        total = pair[k, row_own, :].astype(f32) + zgot[k].astype(f32)
+        second_hop(k).wait_recv()
+        total = pair[k, zl if x_first(k) else x].astype(f32) + zgot[k].astype(f32)
         out_ref[mine, columns(k)] = (x_own[:, columns(k)].astype(f32) + 0.5 * total).astype(bf)
         finish(k).start()
 
     order = (0, 2, 1, 3, 4, 6, 5, 7)
     for turn in range(len(order) + 3):
         if turn == 0:
-            relay((3, 2))
+            by_place(relay, ((6, 2),), ((4, 2),))
         if turn == 1:
-            relay((5, 2))
+            by_place(relay, ((7, 2),), ((5, 2),))
         if turn == 2:
             for o in range(4):
                 lend(o, 2).wait_recv()
-            relay((7, 2))
         if turn == 6:
             for o in range(4, 8):
                 lend(o, 2).wait_recv()
@@ -436,13 +487,18 @@
         finish(k).wait_recv()
     for copy in sent:
         copy.wait_send()
+    for d in (2, 3, 1):
+        @pl.when(later[d])
+        def _():
+            total_to(d).wait_send()
+
     for o in range(8):
         for k in range(3):
             if o:
                 direct(o, k).wait_send()
             lend(o, k).wait_send()
     for k in range(8):
-        for copy in (swap(k), across_x(k), across_z(k), finish(k)):
+        for copy in (swap(k), first_hop(k, 0), first_hop(k, 1), second_hop(k), finish(k)):
             copy.wait_send()
 
 
@@ -483,6 +539,8 @@
             pltpu.VMEM((GROUPS, share, 2 * width), bf),
             pltpu.VMEM((model, 2 * width), bf),
             pltpu.VMEM((padded, model), bf),
+            pltpu.VMEM((share, 2 * width), bf),
+            pltpu.VMEM((width, share), bf),
             pltpu.VMEM((length, channels), f32),
             pltpu.VMEM((length, channels), bf),
             pltpu.VMEM((4, message, HD), bf),
@@ -500,13 +558,13 @@
             pltpu.VMEM((chunks, GROUPS * length, tile), bf),
             pltpu.VMEM((chunks, GROUPS * own, tile), bf),
             pltpu.VMEM((chunks, GROUPS * own, tile), bf),
-            pltpu.VMEM((chunks, 2 * own, tile), bf),
-            pltpu.VMEM((chunks, 2 * own, tile), bf),
+            pltpu.VMEM((chunks, 2, own, tile), bf),
+            pltpu.VMEM((chunks, 2, own, tile), bf),
             pltpu.VMEM((chunks, own, tile), bf),
-            dma((10,)), dma((8, 3)), dma((8, 3)), dma((8, 3)), dma((8, 3)),
+            dma((10,)), dma((8, 3)), dma((8, 3)), dma((8, 3)), dma((8, 3)), dma((3,)), dma((3,)),
             dma((3,)), dma((3,)), dma((3,)), dma((3,)), dma((3,)), dma((3,)), dma((1,)), dma((1,)),
             dma((3,)), dma((3,)), dma((4,)), dma((4,)),
-            dma((chunks,)), dma((chunks,)), dma((chunks,)), dma((chunks,)), dma((chunks,)), dma((chunks,)),
+            dma((chunks,)), dma((chunks,)), dma((chunks, 2)), dma((chunks, 2)), dma((chunks,)), dma((chunks,)),
             dma((chunks,)), dma((chunks,)),
         ],
         compiler_params=pltpu.CompilerParams(

time: 168 us -> 145 us (0.86)
  Pallas kernels: 165 us -> 142 us
    pallas_call x1, Pallas kernels: 165 us -> 142 us  [layer(): pl.pallas_call(lambda *refs: layer_kernel(dims, *refs), out_shape=jax.Sha...]
where the time goes in v2:
time: 145 us
  Pallas kernels  142 us (98%)
  local copies, waits for them, and re-layouts  2.3 us (2%)
    pallas_call x1, Pallas kernels, layer(): pl.pallas_call(lambda *refs: layer_kernel(dims, *refs), out_shape=jax.Sha...  142 us

profile of v2, /device:TPU:1, one launch (start us, length us, event | category | flops | bytes accessed | tf_op | source)
XLA Modules:
  0.0 144.6 jit_solution(12537708385495694868)
XLA Ops:
  0.0 142.2 %shard_map.127 = bf16[256,2048]{1,0:T(8,128)(2,1)} custom-call(bf16[128,2816]{1,0:T(8,128)(2,1)} %refs_0_.1, bf16[128,2816]{1,0:T(8,128)(2,1)} %refs_1_.1, bf16[4,704,128]{2,1,0:T(8,128)(2,1)} %bitcast.4, bf16[256,512]{1,0:T(8,128)(2,1)} %refs_3_.1, bf16[256,512]{1,0:T(8,128)(2,1)} %refs_4_.1, bf16[256,512]{1,0:T(8,128)(2,1)} %refs_5_.1, ...), custom_call_target="tpu_custom_call" | custom-call | tf_op jit(solution)/shard_map/pallas_call | solution.py:524
  142.2 2.3 %copy.15 = bf16[256,2048]{1,0:T(8,128)(2,1)} copy(bf16[256,2048]{1,0:T(8,128)(2,1)} %shard_map.127) | data formatting | bytes 2097152

commit v3 on v2

--- a/solution.py
+++ b/solution.py
@@ -192,7 +192,7 @@
     if padded > width:
         dn[pl.ds(width, padded - width), :] = jnp.zeros((padded - width, model), dn.dtype)
     pl.semaphore_wait(barrier, len(partners))
-    by_place(send, ((2, 2),), ((6, 2), (2, 2)))
+    by_place(send, ((2, 2),), ((4, 2),))
     send((1, 2))
     relay((0, 2))
     loads[0].wait()
@@ -281,7 +281,7 @@
         def _():
             total_to(d).start()
 
-    by_place(send, ((2, 1),), ((6, 0), (2, 1)))
+    by_place(send, ((2, 1),), ((6, 0), (2, 1), (2, 2)))
     take(2)
     relay((1, 2))
     for d in (2, 3, 1):
@@ -312,8 +312,8 @@
     pass_over(2)
     take_passed(0)
     take(1)
-    by_place(send, ((3, 0), (6, 0)), ((5, 1), (3, 0), (4, 2), (7, 0)))
-    relay((2, 0), (2, 2))
+    by_place(send, ((3, 0),), ((5, 1), (3, 0), (7, 0)))
+    by_place(relay, ((2, 0),), ((2, 0), (2, 2)))
     for n in range(heads):
         cols = slice(n * HD, (n + 1) * HD)
         mixed = grown[:, cols] + over(q_grown[:, cols], inc[n], 1, 1)
@@ -357,27 +357,26 @@
     peers = [rows_over(0)]
 
     take_passed(1)
-    by_place(send, (), ((7, 1),))
+    take_passed(2)
+    by_place(
+        send, ((3, 1), (4, 1), (5, 0), (5, 1), (7, 0), (6, 0), (6, 1), (7, 1), (6, 2), (3, 2), (7, 2), (4, 2), (5, 2)),
+        ((7, 1), (7, 2), (6, 2)),
+    )
     relay((1, 1), (2, 1))
-    by_place(relay, ((4, 0), (4, 1)), ((6, 0), (6, 1)))
-    take_passed(2)
-    by_place(send, (), ((7, 2),))
+    by_place(relay, ((4, 0), (4, 1), (2, 2)), ((6, 0), (6, 1)))
     to_z.wait_recv()
     to_x2 = rows_to(2, 2, place(1), c)
     peers.append(rows_over(2))
-    by_place(
-        send, ((7, 0), (4, 1), (6, 1), (5, 0), (7, 1), (5, 1), (3, 1), (3, 2), (4, 2), (6, 2), (5, 2), (7, 2)),
-        ((3, 1), (3, 2), (5, 2)),
-    )
+    by_place(send, (), ((3, 1), (3, 2), (5, 2)))
     to_x.wait_recv()
     peers.append(rows_over(1))
-    by_place(relay, ((5, 0), (6, 0)), ((4, 0), (7, 0), (3, 0)))
+    by_place(relay, ((4, 2), (5, 0)), ((4, 0), (7, 0), (3, 0)))
     to_x2.wait_recv()
     peers.append(rows_over(3))
-    by_place(relay, ((5, 1), (3, 0)), ((7, 1), (6, 2)))
-    by_place(relay, ((7, 0), (3, 1)), ((4, 1), (7, 2)))
-    by_place(relay, ((6, 1), (7, 1)), ((5, 0), (5, 1), (3, 1)))
-    by_place(relay, ((4, 2), (3, 2)), ())
+    by_place(relay, ((5, 1), (3, 0)), ((3, 1), (4, 1)))
+    by_place(relay, ((3, 1), (7, 0)), ((7, 1), (5, 0)))
+    by_place(relay, ((6, 0), (6, 1), (7, 1)), ((5, 1),))
+    by_place(relay, ((3, 2),), ())
     for copy in peers:
         copy.wait_recv()
     for o in range(8):
@@ -402,7 +401,7 @@
             hid[rows, even:] = (both * jax.nn.sigmoid(both) * pltpu.roll(both, 64, 1)).astype(bf)
 
     gate_up(0)
-    by_place(relay, ((5, 2),), ((3, 2),))
+    by_place(relay, ((6, 2),), ((3, 2),))
     gate_up(1)
     loads[9].wait()
 
@@ -466,9 +465,9 @@
     order = (0, 2, 1, 3, 4, 6, 5, 7)
     for turn in range(len(order) + 3):
         if turn == 0:
-            by_place(relay, ((6, 2),), ((4, 2),))
+            by_place(relay, ((7, 2),), ((4, 2),))
         if turn == 1:
-            by_place(relay, ((7, 2),), ((5, 2),))
+            by_place(relay, ((5, 2),), ((5, 2), (7, 2), (6, 2)))
         if turn == 2:
             for o in range(4):
                 lend(o, 2).wait_recv()

time: 145 us -> 143 us (0.986)
  no operation moved by 1% of the time
where the time goes in v3:
time: 143 us
  Pallas kernels  141 us (99%)
  local copies, waits for them, and re-layouts  2.3 us (2%)
    pallas_call x1, Pallas kernels, layer(): pl.pallas_call(lambda *refs: layer_kernel(dims, *refs), out_shape=jax.Sha...  141 us

profile of v3, /device:TPU:1, one launch (start us, length us, event | category | flops | bytes accessed | tf_op | source)
XLA Modules:
  0.0 143.1 jit_solution(716378456440781596)
XLA Ops:
  0.0 140.8 %shard_map.127 = bf16[256,2048]{1,0:T(8,128)(2,1)} custom-call(bf16[128,2816]{1,0:T(8,128)(2,1)} %refs_0_.1, bf16[128,2816]{1,0:T(8,128)(2,1)} %refs_1_.1, bf16[4,704,128]{2,1,0:T(8,128)(2,1)} %bitcast.4, bf16[256,512]{1,0:T(8,128)(2,1)} %refs_3_.1, bf16[256,512]{1,0:T(8,128)(2,1)} %refs_4_.1, bf16[256,512]{1,0:T(8,128)(2,1)} %refs_5_.1, ...), custom_call_target="tpu_custom_call" | custom-call | tf_op jit(solution)/shard_map/pallas_call | solution.py:523
  140.8 2.3 %copy.15 = bf16[256,2048]{1,0:T(8,128)(2,1)} copy(bf16[256,2048]{1,0:T(8,128)(2,1)} %shard_map.127) | data formatting | bytes 2097152
